TPU v7x, 512 devices: a 8x2x16 block of a 8x8x16 slice. The times are simulated.
512 devices in a mesh: grp: 2 (over y), dp: 8 (over x), kv: 16 (over z), tp: 2 (over core).
Axes of the slice: x: 8, y: 2, z: 16, core: 2. Of those that a mesh axis runs over, the one named last changes fastest.
The devices are a block of a 8x8x16 slice.
Arguments:
- inputs: bfloat16 [512, 4096], P(('grp', 'dp'), 'kv'), parts along dimension 0, may hold values from -6 to 6
- gain_in: float32 [4096], P('kv'), may hold values from 0.1 to 1.9
- w_gate: bfloat16 [4096, 2048], P('kv', 'tp'), may hold values from -0.09375 to 0.09375
- w_input: bfloat16 [4096, 2048], P('kv', 'tp'), may hold values from -0.09375 to 0.09375
- w_bproj: bfloat16 [4096, 1024], P('kv', 'tp'), may hold values from -0.09375 to 0.09375
- w_cproj: bfloat16 [4096, 1024], P('kv', 'tp'), may hold values from -0.09375 to 0.09375
- w_step: bfloat16 [4096, 32], P('kv', 'tp'), may hold values from -0.09375 to 0.09375
- conv_input: float32 [4, 2048], P(None, 'tp'), may hold values from -3 to 3
- conv_bproj: float32 [4, 1024], P(None, 'tp'), may hold values from -3 to 3
- conv_cproj: float32 [4, 1024], P(None, 'tp'), may hold values from -3 to 3
- tail_input: bfloat16 [512, 3, 2048], P(('grp', 'dp', 'kv'), None, 'tp'), parts along dimension 0, may hold values from -6 to 6
- tail_bproj: bfloat16 [512, 3, 1024], P(('grp', 'dp', 'kv'), None, 'tp'), parts along dimension 0, may hold values from -6 to 6
- tail_cproj: bfloat16 [512, 3, 1024], P(('grp', 'dp', 'kv'), None, 'tp'), parts along dimension 0, may hold values from -6 to 6
- step_bias: float32 [32], P('tp'), may hold values from -3 to 0
- decay_log: float32 [32], P('tp'), may hold values from -2 to 2
- block_input: bfloat16 [512, 128, 2048], P(('grp', 'dp', 'kv'), None, 'tp'), parts along dimension 0, may hold values from -6 to 6
- block_bproj: bfloat16 [512, 128, 1024], P(('grp', 'dp', 'kv'), None, 'tp'), parts along dimension 0, may hold values from -0.59765625 to 0.59765625
- block_step: float32 [512, 128, 32], P(('grp', 'dp', 'kv'), None, 'tp'), parts along dimension 0, may hold values from 0.005 to 0.2
- lengths: int32 [512], P(('grp', 'dp', 'kv')), parts along dimension 0, may hold values from 1 to 127, 8192 in all
- state: float32 [512, 32, 64, 128], P(('grp', 'dp', 'kv'), 'tp'), parts along dimension 0, may hold values from -0.6 to 0.6
- gain_mix: float32 [2048], P('tp'), may hold values from 0.1 to 1.9
- w_out: bfloat16 [2048, 4096], P('tp', 'kv'), may hold values from -0.125 to 0.125
- gain_mlp: float32 [4096], P(('kv', 'tp')), may hold values from 0.1 to 1.9
- w_up: bfloat16 [4096, 16384], P(('kv', 'tp'), 'dp'), may hold values from -0.09375 to 0.09375
- w_down: bfloat16 [16384, 4096], P('dp', ('kv', 'tp')), may hold values from -0.046875 to 0.046875
Outputs:
- layer_out: bfloat16 [512, 4096], P(('grp', 'dp'), ('kv', 'tp')), parts along dimension 0
There are 2 independent parts, one for each index of `grp`. A program takes and returns all parts, laid end to end along the dimension named above; an argument that names none is the same for every part. Nothing has to cross between parts.
Inputs may be any that keep to these rules, and one draw needn't show every extreme that they name: `lengths`: the number of live positions before the new token in each sequence's current block; the largest equals 127 in every draw.
All inputs are finite; a program needn't handle non-finite values.
Results may differ from a plain program's by a relative error of at most 0.012.
Values may be sent and summed in bfloat16 or wider, within the bound.
No kernel may reach another device: no remote copies, remote signals or barrier semaphores. Data moves between devices by JAX's collectives and lax.ppermute only.
A program may use at most 64 MiB of HBM per device.

v0:
```python
import jax
import jax.numpy as jnp
from jax import lax
from jax.sharding import PartitionSpec as P

D = 4096
HEAD_DIM = 64
D_STATE = 128
TAPS = 4
SSM_WIDTH = 2048
LANES = 128
EPS = 1e-06
BF16 = jnp.bfloat16
F32 = jnp.float32


def two_words(x):
    high = lax.reduce_precision(x, 8, 7)
    return (high.astype(BF16), (x - high).astype(BF16))


def to_everyone(shard, axes):
    size = lax.axis_size(axes)
    return lax.all_to_all(
        jnp.broadcast_to(shard[None], (size, *shard.shape)), axes, 0, 0, tiled=True
    )


def from_partner(x):
    size = lax.axis_size("tp")
    return lax.ppermute(x, "tp", [(i, (i + 1) % size) for i in range(size)])


def exchanged(weight, dim, core):
    half = weight.shape[dim] // 2
    mine = lax.dynamic_slice_in_dim(weight, core * half, half, dim)
    other = lax.dynamic_slice_in_dim(weight, (1 - core) * half, half, dim)
    return (mine, from_partner(other))


def in_core_order(mine, other, core, dim):
    return jnp.where(
        core == 0,
        jnp.concatenate([mine, other], axis=dim),
        jnp.concatenate([other, mine], axis=dim),
    )


def convolve(history, weights, newest):
    summed = weights[TAPS - 1] * newest
    for offset in range(TAPS - 1):
        summed = summed + weights[offset] * history[:, offset].astype(F32)
    return jax.nn.silu(summed)


def per_device(
    inputs,
    gain_in,
    w_gate,
    w_input,
    w_bproj,
    w_cproj,
    w_step,
    conv_input,
    conv_bproj,
    conv_cproj,
    tail_input,
    tail_bproj,
    tail_cproj,
    step_bias,
    decay_log,
    block_input,
    block_bproj,
    block_step,
    lengths,
    state,
    gain_mix,
    w_out,
    gain_mlp,
    w_up,
    w_down,
):
    core = lax.axis_index("tp")
    n_kv, n_dp, n_tp = (lax.axis_size("kv"), lax.axis_size("dp"), lax.axis_size("tp"))
    stream = inputs.astype(F32)
    rows = inputs.shape[0]
    squares = jnp.sum(stream * stream, axis=1)
    scaled = (stream * gain_in).astype(BF16)
    matrices = (w_gate, w_input, w_bproj, w_cproj)
    pieces = [
        jnp.dot(scaled, weight, preferred_element_type=F32).astype(BF16) for weight in matrices
    ]
    pieces += two_words(jnp.dot(scaled, w_step, preferred_element_type=F32))
    pieces += two_words(squares[:, None])
    bounds = [0]
    for piece in pieces:
        bounds.append(bounds[-1] + piece.shape[1])
    spare = -bounds[-1] % LANES
    pieces.append(jnp.zeros((rows, spare), BF16))
    sent = jnp.concatenate(pieces, axis=1).reshape(n_kv, rows // n_kv, -1)
    arrived = lax.all_to_all(sent, "kv", 0, 0, tiled=True)
    projected = jnp.sum(arrived.astype(F32), axis=0)
    out_mine, out_other = exchanged(w_out, 1, core)
    up_mine, up_other = exchanged(w_up, 1, core)
    down_mine, down_other = exchanged(w_down, 0, core)
    gain_other = from_partner(gain_mlp)
    out_weight = jnp.concatenate([out_mine, out_other], axis=0)
    up_weight = jnp.concatenate([up_mine, up_other], axis=0)
    down_weight = in_core_order(down_mine, down_other, core, 1)
    up_gain = jnp.concatenate([gain_mlp, gain_other])
    parts = [projected[:, a:b] for a, b in zip(bounds[:-1], bounds[1:])]
    inverse = lax.rsqrt((parts[6] + parts[7]) / D + EPS)
    gate_pre, value_pre, b_pre, c_pre = [parts[k] * inverse for k in range(4)]
    step_pre = (parts[4] + parts[5]) * inverse
    seq_count = lengths.shape[0]
    head_count = step_bias.shape[0]
    group_count = w_bproj.shape[1] // D_STATE
    block_len = block_step.shape[1]
    per_group = head_count // group_count
    current = convolve(tail_input, conv_input, value_pre)
    b_now = convolve(tail_bproj, conv_bproj, b_pre)
    c_now = convolve(tail_cproj, conv_cproj, c_pre)
    step_size = jax.nn.softplus(step_pre + step_bias)
    decay_rate = -jnp.exp(decay_log)
    positions = lax.broadcasted_iota(jnp.int32, (1, block_len), 1)
    live_rows = (positions < lengths[:, None]).astype(F32)
    masked = block_step * live_rows[:, :, None]
    later_steps = jnp.sum(masked, axis=1, keepdims=True) - jnp.cumsum(masked, axis=1)
    decays = jnp.exp(decay_rate * (step_size[:, None, :] + later_steps)) * live_rows[:, :, None]
    c_query = c_now.astype(BF16).reshape(seq_count, group_count, D_STATE)
    keys = block_bproj.reshape(seq_count, block_len, group_count, D_STATE)
    scores = jnp.einsum("bsgn,bgn->bsg", keys, c_query, preferred_element_type=F32)
    scores = jnp.repeat(scores, per_group, axis=2)
    weights = (decays * scores * block_step).astype(BF16)
    values = block_input.reshape(seq_count, block_len, head_count, HEAD_DIM)
    inner_sum = jnp.einsum("bsh,bshp->bhp", weights, values, preferred_element_type=F32)
    c_full = c_now.reshape(seq_count, group_count, D_STATE)
    b_full = b_now.reshape(seq_count, group_count, D_STATE)
    own_score = jnp.repeat(jnp.sum(c_full * b_full, axis=2), per_group, axis=1)
    own_term = (step_size * own_score)[:, :, None] * current.reshape(
        seq_count, head_count, HEAD_DIM
    )
    carried = jnp.exp(decay_rate * (step_size + jnp.sum(masked, axis=1)))
    c_heads = jnp.repeat(c_full, per_group, axis=1)
    readout = jnp.einsum("bhpn,bhn->bhp", state, c_heads, precision=lax.Precision.HIGHEST)
    mixed = (inner_sum + own_term + carried[:, :, None] * readout).reshape(
        seq_count, -1
    ) * jax.nn.silu(gate_pre)
    width = mixed.shape[1]
    local_sq = two_words(jnp.sum(mixed * mixed, axis=1, keepdims=True))
    row = jnp.concatenate(
        [(mixed * gain_mix).astype(BF16), *local_sq, jnp.zeros((seq_count, LANES - 2), BF16)],
        axis=1,
    )
    whole = to_everyone(row, ("kv", "tp")).reshape(n_kv, n_tp, seq_count, -1)
    whole = jnp.moveaxis(whole, 1, 0).reshape(n_tp, rows, -1)
    total_sq = jnp.sum(whole[:, :, width : width + 2].astype(F32), axis=(0, 2))
    halves = whole[:, :, :width]
    channels = jnp.concatenate(
        [
            lax.dynamic_index_in_dim(halves, core, 0, keepdims=False),
            lax.dynamic_index_in_dim(halves, 1 - core, 0, keepdims=False),
        ],
        axis=1,
    )
    mixed_in = jnp.dot(channels, out_weight, preferred_element_type=F32)
    mixed_in = mixed_in * lax.rsqrt(total_sq / SSM_WIDTH + EPS)[:, None]
    column_count = mixed_in.shape[1]
    residual = lax.dynamic_slice_in_dim(stream, core * column_count, column_count, 1)
    hidden = (residual + mixed_in).astype(BF16)
    all_hidden = to_everyone(hidden, ("dp", "tp")).reshape(n_dp, n_tp, rows, -1)
    all_hidden = jnp.moveaxis(all_hidden, 1, 0).reshape(n_tp, n_dp * rows, -1)
    all_hidden = jnp.concatenate(
        [
            lax.dynamic_index_in_dim(all_hidden, core, 0, keepdims=False),
            lax.dynamic_index_in_dim(all_hidden, 1 - core, 0, keepdims=False),
        ],
        axis=1,
    ).astype(F32)
    row_sq = jnp.sum(all_hidden * all_hidden, axis=1)
    lifted = (all_hidden * up_gain).astype(BF16)
    raised = lax.dot_general(
        up_weight, lifted, (((0,), (1,)), ((), ())), preferred_element_type=F32
    ).astype(BF16)
    seqs = raised.shape[1]
    extra = jnp.concatenate(
        [*[w[None] for w in two_words(row_sq)], jnp.zeros((6, seqs), BF16)], axis=0
    )
    sent = jnp.concatenate(
        [raised.reshape(n_kv, -1, seqs), jnp.broadcast_to(extra[None], (n_kv, *extra.shape))],
        axis=1,
    )
    arrived = lax.all_to_all(sent, "kv", 0, 0, tiled=True)
    shares = jnp.sum(arrived.astype(F32), axis=0)
    unit_count = shares.shape[0] - 8
    sq_sum = shares[unit_count] + shares[unit_count + 1]
    units = jnp.square(
        jax.nn.relu(shares[:unit_count] * lax.rsqrt(sq_sum / D + EPS)[None, :])
    ).astype(BF16)
    hidden_units = lax.all_gather(units, "kv", axis=0, tiled=True)
    lowered = lax.dot_general(
        hidden_units, down_weight, (((0,), (0,)), ((), ())), preferred_element_type=F32
    ).astype(BF16)
    lowered = lowered.reshape(n_dp, rows, n_tp, -1)
    lowered = jnp.moveaxis(lowered, 2, 1).reshape(n_dp * n_tp, rows, -1)
    lowered = lax.all_to_all(lowered, ("dp", "tp"), 0, 0, tiled=True)
    return (hidden.astype(F32) + jnp.sum(lowered.astype(F32), axis=0)).astype(BF16)


def solution(mesh):
    return jax.shard_map(
        per_device,
        mesh=mesh,
        in_specs=(
            P(("grp", "dp"), "kv"),
            P("kv"),
            P("kv", "tp"),
            P("kv", "tp"),
            P("kv", "tp"),
            P("kv", "tp"),
            P("kv", "tp"),
            P(None, "tp"),
            P(None, "tp"),
            P(None, "tp"),
            P(("grp", "dp", "kv"), None, "tp"),
            P(("grp", "dp", "kv"), None, "tp"),
            P(("grp", "dp", "kv"), None, "tp"),
            P("tp"),
            P("tp"),
            P(("grp", "dp", "kv"), None, "tp"),
            P(("grp", "dp", "kv"), None, "tp"),
            P(("grp", "dp", "kv"), None, "tp"),
            P(("grp", "dp", "kv")),
            P(("grp", "dp", "kv"), "tp", None, None),
            P("tp"),
            P("tp", "kv"),
            P(("kv", "tp")),
            P(("kv", "tp"), "dp"),
            P("dp", ("kv", "tp")),
        ),
        out_specs=P(("grp", "dp"), ("kv", "tp")),
        check_vma=False,
    )
```

profile of v0, /device:TPU:65, one launch (start us, length us, event | category | flops | bytes accessed | tf_op | source)
XLA Modules:
  0.0 200.1 jit_solution(6419792693657834448)
XLA Ops:
  0.0 0.9 multiply_reduce_fusion
  1.4 0.9 fusion.26
  2.4 1.1 convolution_convert_fusion.5
  3.6 1.1 convolution_convert_fusion.4
  4.8 1.3 convolution_convert_fusion.3
  6.4 1.1 concatenate.52
  7.5 44.2 %all-to-all-start = ((bf16[16,2,3200]{2,1,0:T(2,128)(2,1)}), bf16[16,2,3200]{2,1,0:T(2,128)(2,1)S(1)}, u32[]{:S(2)}, u32[]{:S(2)}) async-start(bf16[16,2,3200]{2,1,0:T(2,128)(2,1)} %concatenate.52), calls=%async_computation | async-start | bytes 409600 | tf_op jit(solution)/shard_map/all_to_all | solution.py:101
  52.3 0.3 copy.67
  52.9 11.0 %all-to-all-done = bf16[16,2,3200]{2,1,0:T(2,128)(2,1)S(1)} async-done(((bf16[16,2,3200]{2,1,0:T(2,128)(2,1)}), bf16[16,2,3200]{2,1,0:T(2,128)(2,1)S(1)}, u32[]{:S(2)}, u32[]{:S(2)}) %all-to-all-start) | async-done | bytes 204832 | tf_op jit(solution)/shard_map/all_to_all | solution.py:101
  65.5 1.7 fusion.62
  67.3 0.4 fusion.61
  68.3 0.8 broadcast_in_dim.23
  69.0 10.6 %all-to-all-start.1 = ((bf16[32,2,1152]{2,1,0:T(2,128)(2,1)}), bf16[32,2,1152]{2,1,0:T(2,128)(2,1)S(1)}, u32[]{:S(2)}, u32[]{:S(2)}) async-start(bf16[32,2,1152]{2,1,0:T(2,128)(2,1)} %broadcast_in_dim.23), calls=%async_computation.1 | async-start | bytes 294912 | tf_op jit(solution)/shard_map/all_to_all | solution.py:24
  79.7 2.6 %collective-permute-start = (bf16[1024,128]{1,0:T(8,128)(2,1)S(1)}, bf16[1024,128]{1,0:T(8,128)(2,1)S(1)}, u32[]{:S(2)}, u32[]{:S(2)}) collective-permute-start(bf16[1024,128]{1,0:T(8,128)(2,1)S(1)} %get-tuple-element.18), channel_id=1, source_target_pairs={{0,1},{1,0},{2,3},{3,2},{4,5},{5,4},{6,7},{7,6},{8,9},{9,8},{10,11... | collective-permute-start | bytes 786440 | tf_op jit(solution)/shard_map/ppermute | solution.py:31
  82.3 13.6 %all-to-all-done.1 = bf16[32,2,1152]{2,1,0:T(2,128)(2,1)S(1)} async-done(((bf16[32,2,1152]{2,1,0:T(2,128)(2,1)}), bf16[32,2,1152]{2,1,0:T(2,128)(2,1)S(1)}, u32[]{:S(2)}, u32[]{:S(2)}) %all-to-all-start.1) | async-done | bytes 147488 | tf_op jit(solution)/shard_map/all_to_all | solution.py:24
  96.0 0.3 convert_reduce_fusion.3
  96.5 0.3 constant_dynamic-slice_fusion.7
  96.8 0.2 fusion.1
  97.1 0.7 broadcast_in_dim.24
  97.7 8.9 %all-to-all-start.2 = ((bf16[16,32,128]{2,1,0:T(8,128)(2,1)}), bf16[16,32,128]{2,1,0:T(8,128)(2,1)S(1)}, u32[]{:S(2)}, u32[]{:S(2)}) async-start(bf16[16,32,128]{2,1,0:T(8,128)(2,1)} %broadcast_in_dim.24), calls=%async_computation.2 | async-start | bytes 262144 | tf_op jit(solution)/shard_map/all_to_all | solution.py:24
  106.6 2.2 %collective-permute-start.2 = (f32[128]{0:T(128)S(1)}, f32[128]{0:T(128)S(1)}, u32[]{:S(2)}, u32[]{:S(2)}) collective-permute-start(f32[128]{0:T(128)S(1)} %copy-done.18), channel_id=1, source_target_pairs={{0,1},{1,0},{2,3},{3,2},{4,5},{5,4},{6,7},{7,6},{8,9},{9,8},{10,11... | collective-permute-start | bytes 1544 | tf_op jit(solution)/shard_map/ppermute | solution.py:31
  109.0 2.1 %collective-permute-start.1 = (bf16[128,1024]{1,0:T(8,128)(2,1)S(1)}, bf16[128,1024]{1,0:T(8,128)(2,1)S(1)}, u32[]{:S(2)}, u32[]{:S(2)}) collective-permute-start(bf16[128,1024]{1,0:T(8,128)(2,1)S(1)} %get-tuple-element.16), channel_id=1, source_target_pairs={{0,1},{1,0},{2,3},{3,2},{4,5},{5,4},{6,7},{7,6},{8,9},{9,8},{10,11... | collective-permute-start | bytes 786440 | tf_op jit(solution)/shard_map/ppermute | solution.py:31
  111.2 4.3 %all-to-all-done.2 = bf16[16,32,128]{2,1,0:T(8,128)(2,1)S(1)} async-done(((bf16[16,32,128]{2,1,0:T(8,128)(2,1)}), bf16[16,32,128]{2,1,0:T(8,128)(2,1)S(1)}, u32[]{:S(2)}, u32[]{:S(2)}) %all-to-all-start.2) | async-done | bytes 131104 | tf_op jit(solution)/shard_map/all_to_all | solution.py:24
  115.8 0.4 convolution_convert_fusion
  116.2 0.9 pad_maximum_fusion
  117.0 4.0 %all-to-all-start.3 = ((bf16[16,72,256]{2,1,0:T(8,128)(2,1)}), bf16[16,72,256]{2,1,0:T(8,128)(2,1)S(1)}, u32[]{:S(2)}, u32[]{:S(2)}) async-start(bf16[16,72,256]{2,1,0:T(8,128)(2,1)} %pad_maximum_fusion), calls=%async_computation.3 | async-start | bytes 1179648 | tf_op jit(solution)/shard_map/all_to_all | solution.py:193
  121.1 2.0 collective-permute-start.3
  123.1 26.3 %all-to-all-done.3 = bf16[16,72,256]{2,1,0:T(8,128)(2,1)S(1)} async-done(((bf16[16,72,256]{2,1,0:T(8,128)(2,1)}), bf16[16,72,256]{2,1,0:T(8,128)(2,1)S(1)}, u32[]{:S(2)}, u32[]{:S(2)}) %all-to-all-start.3) | async-done | bytes 589856 | tf_op jit(solution)/shard_map/all_to_all | solution.py:193
  149.5 27.8 %all_gather.3 = bf16[1024,256]{1,0:T(8,128)(2,1)S(1)} all-gather(bf16[64,256]{1,0:T(8,128)(2,1)S(1)} %fusion.24), channel_id=1, replica_groups=mesh['grp'=2,'dp'=8,'kv'=16,'tp'=2] {'kv'}, dimensions={0}, use_global_device_ids=true | all-gather | bytes 557056 | tf_op jit(solution)/shard_map/all_gather | solution.py:200
  177.3 0.4 convolution_convert_fusion.1
  177.7 21.7 %all_to_all.25 = bf16[16,32,128]{2,1,0:T(8,128)(2,1)S(1)} all-to-all(bf16[16,32,128]{2,1,0:T(8,128)(2,1)S(1)} %bitcast.105), channel_id=1, replica_groups=mesh['grp'=2,'dp'=8,'kv'=16,'tp'=2] {'dp','tp'}, dimensions={0} | all-to-all | bytes 262144 | tf_op jit(solution)/shard_map/all_to_all | solution.py:206
  199.5 0.6 add_convert_fusion
  (118 shorter events, 4.7 us)
Async XLA Ops:
  0.0 65.5 %copy-start = (f32[2,16,64,128]{3,2,1,0:T(8,128)S(1)}, f32[2,16,64,128]{3,2,1,0:T(8,128)}, u32[]{:S(2)}) copy-start(f32[2,16,64,128]{3,2,1,0:T(8,128)} %param.44) | copy-start | bytes 3145732
  0.0 6.1 %copy-start.1 = (bf16[32,256]{1,0:T(8,128)(2,1)S(1)}, bf16[32,256]{1,0:T(8,128)(2,1)}, u32[]{:S(2)}) copy-start(bf16[32,256]{1,0:T(8,128)(2,1)} %param.25) | copy-start | bytes 49156
  0.0 6.1 %copy-start.8 = (f32[256]{0:T(256)S(1)}, f32[256]{0:T(256)}, u32[]{:S(2)}) copy-start(f32[256]{0:T(256)} %param.26) | copy-start | bytes 3076
  0.0 6.1 %copy-start.5 = (bf16[256,1024]{1,0:T(8,128)(2,1)S(1)}, bf16[256,1024]{1,0:T(8,128)(2,1)}, u32[]{:S(2)}) copy-start(bf16[256,1024]{1,0:T(8,128)(2,1)} %param.28) | copy-start | bytes 1572868
  4.7 47.0 %copy-start.19 = (s32[2]{0:T(128)S(1)}, s32[2]{0:T(128)}, u32[]{:S(2)}) copy-start(s32[2]{0:T(128)} %param.43) | copy-start | bytes 28
  4.8 47.1 %copy-start.9 = (f32[2,128,16]{1,2,0:T(8,128)S(1)}, f32[2,128,16]{1,2,0:T(8,128)}, u32[]{:S(2)}) copy-start(f32[2,128,16]{1,2,0:T(8,128)} %param.42) | copy-start | bytes 49156
  6.0 46.0 %copy-start.20 = (f32[16]{0:T(128)S(1)}, f32[16]{0:T(128)}, u32[]{:S(2)}) copy-start(f32[16]{0:T(128)} %param.39) | copy-start | bytes 196
  6.1 46.0 %copy-start.7 = (bf16[2,128,512]{2,1,0:T(8,128)(2,1)S(1)}, bf16[2,128,512]{2,1,0:T(8,128)(2,1)}, u32[]{:S(2)}) copy-start(bf16[2,128,512]{2,1,0:T(8,128)(2,1)} %param.41) | copy-start | bytes 786436
  6.3 46.0 %copy-start.6 = (bf16[2,128,1024]{2,1,0:T(8,128)(2,1)S(1)}, bf16[2,128,1024]{2,1,0:T(8,128)(2,1)}, u32[]{:S(2)}) copy-start(bf16[2,128,1024]{2,1,0:T(8,128)(2,1)} %param.40) | copy-start | bytes 1572868
  7.5 56.4 %all-to-all-start = ((bf16[16,2,3200]{2,1,0:T(2,128)(2,1)}), bf16[16,2,3200]{2,1,0:T(2,128)(2,1)S(1)}, u32[]{:S(2)}, u32[]{:S(2)}) async-start(bf16[16,2,3200]{2,1,0:T(2,128)(2,1)} %concatenate.52), calls=%async_computation | async-start | bytes 409600 | tf_op jit(solution)/shard_map/all_to_all | solution.py:101
  51.9 0.9 copy-start.12
  51.9 0.9 copy-start.13
  52.0 0.9 copy-start.10
  52.1 12.2 %copy-start.14 = (bf16[2,3,512]{2,0,1:T(2,128)(2,1)S(1)}, bf16[2,3,512]{2,0,1:T(2,128)(2,1)}, u32[]{:S(2)}) copy-start(bf16[2,3,512]{2,0,1:T(2,128)(2,1)} %param.37) | copy-start | bytes 18436
  52.1 12.2 %copy-start.15 = (bf16[2,3,512]{2,0,1:T(2,128)(2,1)S(1)}, bf16[2,3,512]{2,0,1:T(2,128)(2,1)}, u32[]{:S(2)}) copy-start(bf16[2,3,512]{2,0,1:T(2,128)(2,1)} %param.36) | copy-start | bytes 18436
  52.1 12.6 %copy-start.11 = (bf16[2,3,1024]{2,0,1:T(2,128)(2,1)S(1)}, bf16[2,3,1024]{2,0,1:T(2,128)(2,1)}, u32[]{:S(2)}) copy-start(bf16[2,3,1024]{2,0,1:T(2,128)(2,1)} %param.35) | copy-start | bytes 36868
  52.3 12.8 %copy-start.17 = (f32[16]{0:T(128)S(1)}, f32[16]{0:T(128)}, u32[]{:S(2)}) copy-start(f32[16]{0:T(128)} %param.38) | copy-start | bytes 196
  65.4 2.7 %copy-start.16 = (f32[1024]{0:T(1024)S(1)}, f32[1024]{0:T(1024)}, u32[]{:S(2)}) copy-start(f32[1024]{0:T(1024)} %param.45) | copy-start | bytes 12292
  65.5 14.1 %copy-start.2 = (bf16[1024,256]{1,0:T(8,128)(2,1)S(1)}, bf16[1024,256]{1,0:T(8,128)(2,1)}, u32[]{:S(2)}) copy-start(bf16[1024,256]{1,0:T(8,128)(2,1)} %param.46) | copy-start | bytes 1572868
  69.0 26.9 %all-to-all-start.1 = ((bf16[32,2,1152]{2,1,0:T(2,128)(2,1)}), bf16[32,2,1152]{2,1,0:T(2,128)(2,1)S(1)}, u32[]{:S(2)}, u32[]{:S(2)}) async-start(bf16[32,2,1152]{2,1,0:T(2,128)(2,1)} %broadcast_in_dim.23), calls=%async_computation.1 | async-start | bytes 294912 | tf_op jit(solution)/shard_map/all_to_all | solution.py:24
  79.7 17.2 %collective-permute-start = (bf16[1024,128]{1,0:T(8,128)(2,1)S(1)}, bf16[1024,128]{1,0:T(8,128)(2,1)S(1)}, u32[]{:S(2)}, u32[]{:S(2)}) collective-permute-start(bf16[1024,128]{1,0:T(8,128)(2,1)S(1)} %get-tuple-element.18), channel_id=1, source_target_pairs={{0,1},{1,0},{2,3},{3,2},{4,5},{5,4},{6,7},{7,6},{8,9},{9,8},{10,11... | collective-permute-start | bytes 786440 | tf_op jit(solution)/shard_map/ppermute | solution.py:31
  96.7 9.9 %copy-start.18 = (f32[128]{0:T(128)S(1)}, f32[128]{0:T(128)}, u32[]{:S(2)}) copy-start(f32[128]{0:T(128)} %param.47) | copy-start | bytes 1540
  96.8 12.1 %copy-start.3 = (bf16[128,2048]{1,0:T(8,128)(2,1)S(1)}, bf16[128,2048]{1,0:T(8,128)(2,1)}, u32[]{:S(2)}) copy-start(bf16[128,2048]{1,0:T(8,128)(2,1)} %param.48) | copy-start | bytes 1572868
  97.7 17.8 %all-to-all-start.2 = ((bf16[16,32,128]{2,1,0:T(8,128)(2,1)}), bf16[16,32,128]{2,1,0:T(8,128)(2,1)S(1)}, u32[]{:S(2)}, u32[]{:S(2)}) async-start(bf16[16,32,128]{2,1,0:T(8,128)(2,1)} %broadcast_in_dim.24), calls=%async_computation.2 | async-start | bytes 262144 | tf_op jit(solution)/shard_map/all_to_all | solution.py:24
  106.6 4.6 %collective-permute-start.2 = (f32[128]{0:T(128)S(1)}, f32[128]{0:T(128)S(1)}, u32[]{:S(2)}, u32[]{:S(2)}) collective-permute-start(f32[128]{0:T(128)S(1)} %copy-done.18), channel_id=1, source_target_pairs={{0,1},{1,0},{2,3},{3,2},{4,5},{5,4},{6,7},{7,6},{8,9},{9,8},{10,11... | collective-permute-start | bytes 1544 | tf_op jit(solution)/shard_map/ppermute | solution.py:31
  109.0 6.8 %collective-permute-start.1 = (bf16[128,1024]{1,0:T(8,128)(2,1)S(1)}, bf16[128,1024]{1,0:T(8,128)(2,1)S(1)}, u32[]{:S(2)}, u32[]{:S(2)}) collective-permute-start(bf16[128,1024]{1,0:T(8,128)(2,1)S(1)} %get-tuple-element.16), channel_id=1, source_target_pairs={{0,1},{1,0},{2,3},{3,2},{4,5},{5,4},{6,7},{7,6},{8,9},{9,8},{10,11... | collective-permute-start | bytes 786440 | tf_op jit(solution)/shard_map/ppermute | solution.py:31
  116.1 4.9 %copy-start.4 = (bf16[2048,128]{1,0:T(8,128)(2,1)S(1)}, bf16[2048,128]{1,0:T(8,128)(2,1)}, u32[]{:S(2)}) copy-start(bf16[2048,128]{1,0:T(8,128)(2,1)} %param.49) | copy-start | bytes 1572868
  117.0 32.4 %all-to-all-start.3 = ((bf16[16,72,256]{2,1,0:T(8,128)(2,1)}), bf16[16,72,256]{2,1,0:T(8,128)(2,1)S(1)}, u32[]{:S(2)}, u32[]{:S(2)}) async-start(bf16[16,72,256]{2,1,0:T(8,128)(2,1)} %pad_maximum_fusion), calls=%async_computation.3 | async-start | bytes 1179648 | tf_op jit(solution)/shard_map/all_to_all | solution.py:193
  121.1 56.2 %collective-permute-start.3 = (bf16[1024,128]{1,0:T(8,128)(2,1)S(1)}, bf16[1024,128]{1,0:T(8,128)(2,1)S(1)}, u32[]{:S(2)}, u32[]{:S(2)}) collective-permute-start(bf16[1024,128]{1,0:T(8,128)(2,1)S(1)} %get-tuple-element.14), channel_id=1, source_target_pairs={{0,1},{1,0},{2,3},{3,2},{4,5},{5,4},{6,7},{7,6},{8,9},{9,8},{10,11... | collective-permute-start | bytes 786440 | tf_op jit(solution)/shard_map/ppermute | solution.py:31
where the time goes:
time: 201 us; the launch traced here: 200 us
  starting transfers between devices  76.7 us (38%)
  waiting for transfers between devices  55.3 us (28%)
  blocking collectives  49.5 us (25%)
  matrix products  7.82 us (4%)
  local copies, waits for them, and re-layouts  5.53 us (3%)
  other arithmetic  4.62 us (2%)
    all_to_all x2, starting transfers between devices, per_device(): arrived = lax.all_to_all(sent, 'kv', 0, 0, tiled=True)  48.2 us
    all_to_all x2, waiting for transfers between devices, per_device(): arrived = lax.all_to_all(sent, 'kv', 0, 0, tiled=True)  37.3 us
    all_gather x1, blocking collectives, per_device(): hidden_units = lax.all_gather(units, 'kv', axis=0, tiled=True)  27.8 us
    all_to_all x1, blocking collectives, per_device(): lowered = lax.all_to_all(lowered, ('dp', 'tp'), 0, 0, tiled=True)  21.7 us
    all_to_all x2, starting transfers between devices, to_everyone(): lax.all_to_all(jnp.broadcast_to(shard[None], (size, *shard.shape)), axes,...  19.5 us
    all_to_all x2, waiting for transfers between devices, to_everyone(): lax.all_to_all(jnp.broadcast_to(shard[None], (size, *shard.shape)), axes,...  17.9 us
    ppermute x4, starting transfers between devices, from_partner(): return lax.ppermute(x, 'tp', [(i, (i + 1) % size) for i in range(size)])  8.98 us
  transfers between devices with their start and end apart: 8, of which 4 were waited for; matrix products, arithmetic and copies ran while one was open for 1% of the time, Pallas kernels for 0%

commit v1 on v0

--- a/solution.py
+++ b/solution.py
@@ -197,7 +197,16 @@
     units = jnp.square(
         jax.nn.relu(shares[:unit_count] * lax.rsqrt(sq_sum / D + EPS)[None, :])
     ).astype(BF16)
-    hidden_units = lax.all_gather(units, "kv", axis=0, tiled=True)
+    ways = lax.axis_size("kv")
+    up = [(d, (d + 1) % ways) for d in range(ways)]
+    down = [(d, (d - 1) % ways) for d in range(ways)]
+    earlier, later = ([units], [units])
+    for _ in range(ways // 2):
+        earlier.append(lax.ppermute(earlier[-1], "kv", up))
+    for _ in range((ways - 1) // 2):
+        later.append(lax.ppermute(later[-1], "kv", down))
+    line = jnp.concatenate([*earlier[::-1], *later[1:]], axis=0)
+    hidden_units = jnp.roll(line, (lax.axis_index("kv") - ways // 2) * units.shape[0], axis=0)
     lowered = lax.dot_general(
         hidden_units, down_weight, (((0,), (0,)), ((), ())), preferred_element_type=F32
     ).astype(BF16)

time: 201 us -> 230 us (1.14)
  starting transfers between devices: 76.7 us -> 128 us
  waiting for transfers between devices: 55.3 us -> 32.5 us
    ppermute x0 -> x15, starting transfers between devices: none -> 49.3 us  [the longest x7 32.5 us: per_device(): later.append(lax.ppermute(later[-1], 'kv', down))]
    all_to_all x0 -> x1, blocking collectives: none -> 36.9 us  [per_device(): arrived = lax.all_to_all(sent, 'kv', 0, 0, tiled=True)]
    all_gather x1 -> x0, blocking collectives: 27.8 us -> none  [per_device(): hidden_units = lax.all_gather(units, 'kv', axis=0, tiled=True)]
    all_to_all x2 -> x1, waiting for transfers between devices: 37.3 us -> 11.1 us  [per_device(): arrived = lax.all_to_all(sent, 'kv', 0, 0, tiled=True)]
    all_to_all x1, blocking collectives: 21.7 us -> 13.4 us  [per_device(): lowered = lax.all_to_all(lowered, ('dp', 'tp'), 0, 0, tiled=True)]
    ppermute x4, starting transfers between devices: 8.98 us -> 14.9 us  [from_partner(): return lax.ppermute(x, 'tp', [(i, (i + 1) % size) for i in range(size)])]
    all_to_all x2 -> x1, starting transfers between devices: 48.2 us -> 44.2 us  [per_device(): arrived = lax.all_to_all(sent, 'kv', 0, 0, tiled=True)]
    ppermute x0 -> x15, waiting for transfers between devices: none -> 3.54 us  [the longest x8 2.73 us: per_device(): earlier.append(lax.ppermute(earlier[-1], 'kv', up))]
  transfers between devices with their start and end apart: 8 -> 22, of which waited for: 4 -> 5; matrix products, arithmetic and copies ran while one was open for 1% -> 1% of each run, Pallas kernels for 0% -> 0%
where the time goes in v1:
time: 230 us; the launch traced here: 228 us
  starting transfers between devices  128 us (56%)
  blocking collectives  50.3 us (22%)
  waiting for transfers between devices  32.5 us (14%)
  matrix products  6.95 us (3%)
  local copies, waits for them, and re-layouts  5.65 us (2%)
  other arithmetic  3.83 us (2%)
    all_to_all x1, starting transfers between devices, per_device(): arrived = lax.all_to_all(sent, 'kv', 0, 0, tiled=True)  44.2 us
    all_to_all x1, blocking collectives, per_device(): arrived = lax.all_to_all(sent, 'kv', 0, 0, tiled=True)  36.9 us
    ppermute x7, starting transfers between devices, per_device(): later.append(lax.ppermute(later[-1], 'kv', down))  32.5 us
    all_to_all x2, starting transfers between devices, to_everyone(): lax.all_to_all(jnp.broadcast_to(shard[None], (size, *shard.shape)), axes,...  19.5 us
    all_to_all x2, waiting for transfers between devices, to_everyone(): lax.all_to_all(jnp.broadcast_to(shard[None], (size, *shard.shape)), axes,...  17.9 us
    ppermute x8, starting transfers between devices, per_device(): earlier.append(lax.ppermute(earlier[-1], 'kv', up))  16.8 us
    ppermute x4, starting transfers between devices, from_partner(): return lax.ppermute(x, 'tp', [(i, (i + 1) % size) for i in range(size)])  14.9 us
    all_to_all x1, blocking collectives, per_device(): lowered = lax.all_to_all(lowered, ('dp', 'tp'), 0, 0, tiled=True)  13.4 us
  transfers between devices with their start and end apart: 22, of which 5 were waited for; matrix products, arithmetic and copies ran while one was open for 1% of the time, Pallas kernels for 0%

profile of v1, /device:TPU:65, one launch (start us, length us, event | category | flops | bytes accessed | tf_op | source)
XLA Modules:
  0.0 228.3 jit_solution(8083758147317969679)
XLA Ops:
  2.4 1.3 convolution_convert_fusion.3
  3.7 1.3 convolution_convert_fusion.2
  5.5 1.1 concatenate.58
  6.7 44.2 %all-to-all-start = ((bf16[16,2,3200]{2,1,0:T(2,128)(2,1)}), bf16[16,2,3200]{2,1,0:T(2,128)(2,1)S(1)}, u32[]{:S(2)}, u32[]{:S(2)}) async-start(bf16[16,2,3200]{2,1,0:T(2,128)(2,1)} %concatenate.58), calls=%async_computation | async-start | bytes 409600 | tf_op jit(solution)/shard_map/all_to_all | solution.py:101
  52.0 11.1 %all-to-all-done = bf16[16,2,3200]{2,1,0:T(2,128)(2,1)S(1)} async-done(((bf16[16,2,3200]{2,1,0:T(2,128)(2,1)}), bf16[16,2,3200]{2,1,0:T(2,128)(2,1)S(1)}, u32[]{:S(2)}, u32[]{:S(2)}) %all-to-all-start) | async-done | bytes 204832 | tf_op jit(solution)/shard_map/all_to_all | solution.py:101
  65.0 1.8 fusion.64
  68.1 10.6 %all-to-all-start.1 = ((bf16[32,2,1152]{2,1,0:T(2,128)(2,1)}), bf16[32,2,1152]{2,1,0:T(2,128)(2,1)S(1)}, u32[]{:S(2)}, u32[]{:S(2)}) async-start(bf16[32,2,1152]{2,1,0:T(2,128)(2,1)} %broadcast_in_dim.23), calls=%async_computation.1 | async-start | bytes 294912 | tf_op jit(solution)/shard_map/all_to_all | solution.py:24
  78.8 2.6 %collective-permute-start = (bf16[1024,128]{1,0:T(8,128)(2,1)S(1)}, bf16[1024,128]{1,0:T(8,128)(2,1)S(1)}, u32[]{:S(2)}, u32[]{:S(2)}) collective-permute-start(bf16[1024,128]{1,0:T(8,128)(2,1)S(1)} %get-tuple-element.16), channel_id=1, source_target_pairs={{0,1},{1,0},{2,3},{3,2},{4,5},{5,4},{6,7},{7,6},{8,9},{9,8},{10,11... | collective-permute-start | bytes 786440 | tf_op jit(solution)/shard_map/ppermute | solution.py:31
  81.4 13.6 %all-to-all-done.1 = bf16[32,2,1152]{2,1,0:T(2,128)(2,1)S(1)} async-done(((bf16[32,2,1152]{2,1,0:T(2,128)(2,1)}), bf16[32,2,1152]{2,1,0:T(2,128)(2,1)S(1)}, u32[]{:S(2)}, u32[]{:S(2)}) %all-to-all-start.1) | async-done | bytes 147488 | tf_op jit(solution)/shard_map/all_to_all | solution.py:24
  96.8 8.9 %all-to-all-start.2 = ((bf16[16,32,128]{2,1,0:T(8,128)(2,1)}), bf16[16,32,128]{2,1,0:T(8,128)(2,1)S(1)}, u32[]{:S(2)}, u32[]{:S(2)}) async-start(bf16[16,32,128]{2,1,0:T(8,128)(2,1)} %broadcast_in_dim.24), calls=%async_computation.2 | async-start | bytes 262144 | tf_op jit(solution)/shard_map/all_to_all | solution.py:24
  105.8 2.2 collective-permute-start.2
  108.1 2.1 collective-permute-start.1
  110.3 4.3 %all-to-all-done.2 = bf16[16,32,128]{2,1,0:T(8,128)(2,1)S(1)} async-done(((bf16[16,32,128]{2,1,0:T(8,128)(2,1)}), bf16[16,32,128]{2,1,0:T(8,128)(2,1)S(1)}, u32[]{:S(2)}, u32[]{:S(2)}) %all-to-all-start.2) | async-done | bytes 131104 | tf_op jit(solution)/shard_map/all_to_all | solution.py:24
  115.3 36.9 %all_to_all.25 = bf16[16,72,256]{2,1,0:T(8,128)(2,1)S(1)} all-to-all(bf16[16,72,256]{2,1,0:T(8,128)(2,1)S(1)} %pad_maximum_fusion), channel_id=1, replica_groups=mesh['grp'=2,'dp'=8,'kv'=16,'tp'=2] {'kv'}, dimensions={0} | all-to-all | bytes 1179648 | tf_op jit(solution)/shard_map/all_to_all | solution.py:193
  152.3 3.2 %collective-permute-start.3 = (bf16[64,256]{1,0:T(8,128)(2,1)S(1)}, bf16[64,256]{1,0:T(8,128)(2,1)S(1)}, u32[]{:S(2)}, u32[]{:S(2)}) collective-permute-start(bf16[64,256]{1,0:T(8,128)(2,1)S(1)} %fusion.25), channel_id=1, source_target_pairs={{0,2},{2,4},{4,6},{6,8},{8,10},{10,12},{12,14},{14,16},{16,18},{18... | collective-permute-start | bytes 98312 | tf_op jit(solution)/shard_map/ppermute | solution.py:205
  155.5 2.7 %collective-permute-done.3 = bf16[64,256]{1,0:T(8,128)(2,1)S(1)} collective-permute-done((bf16[64,256]{1,0:T(8,128)(2,1)S(1)}, bf16[64,256]{1,0:T(8,128)(2,1)S(1)}, u32[]{:S(2)}, u32[]{:S(2)}) %collective-permute-start.3) | collective-permute-done | bytes 32800 | tf_op jit(solution)/shard_map/ppermute | solution.py:205
  158.2 2.0 collective-permute-start.4
  160.2 4.6 %collective-permute-start.11 = (bf16[64,256]{1,0:T(8,128)(2,1)S(1)}, bf16[64,256]{1,0:T(8,128)(2,1)S(1)}, u32[]{:S(2)}, u32[]{:S(2)}) collective-permute-start(bf16[64,256]{1,0:T(8,128)(2,1)S(1)} %fusion.25), channel_id=1, source_target_pairs={{0,30},{2,0},{4,2},{6,4},{8,6},{10,8},{12,10},{14,12},{16,14},{18,... | collective-permute-start | bytes 98312 | tf_op jit(solution)/shard_map/ppermute | solution.py:207
  164.8 2.0 collective-permute-start.5
  166.8 4.6 %collective-permute-start.12 = (bf16[64,256]{1,0:T(8,128)(2,1)S(1)}, bf16[64,256]{1,0:T(8,128)(2,1)S(1)}, u32[]{:S(2)}, u32[]{:S(2)}) collective-permute-start(bf16[64,256]{1,0:T(8,128)(2,1)S(1)} %collective-permute-done.11), channel_id=1, source_target_pairs={{0,30},{2,0},{4,2},{6,4},{8,6},{10,8},{12,10},{14,12},{16,14},{18,... | collective-permute-start | bytes 98312 | tf_op jit(solution)/shard_map/ppermute | solution.py:207
  171.4 2.0 collective-permute-start.6
  173.4 4.6 %collective-permute-start.13 = (bf16[64,256]{1,0:T(8,128)(2,1)S(1)}, bf16[64,256]{1,0:T(8,128)(2,1)S(1)}, u32[]{:S(2)}, u32[]{:S(2)}) collective-permute-start(bf16[64,256]{1,0:T(8,128)(2,1)S(1)} %collective-permute-done.12), channel_id=1, source_target_pairs={{0,30},{2,0},{4,2},{6,4},{8,6},{10,8},{12,10},{14,12},{16,14},{18,... | collective-permute-start | bytes 98312 | tf_op jit(solution)/shard_map/ppermute | solution.py:207
  178.0 2.0 collective-permute-start.7
  180.0 4.6 %collective-permute-start.14 = (bf16[64,256]{1,0:T(8,128)(2,1)S(1)}, bf16[64,256]{1,0:T(8,128)(2,1)S(1)}, u32[]{:S(2)}, u32[]{:S(2)}) collective-permute-start(bf16[64,256]{1,0:T(8,128)(2,1)S(1)} %collective-permute-done.13), channel_id=1, source_target_pairs={{0,30},{2,0},{4,2},{6,4},{8,6},{10,8},{12,10},{14,12},{16,14},{18,... | collective-permute-start | bytes 98312 | tf_op jit(solution)/shard_map/ppermute | solution.py:207
  184.6 2.0 collective-permute-start.8
  186.5 4.6 %collective-permute-start.15 = (bf16[64,256]{1,0:T(8,128)(2,1)S(1)}, bf16[64,256]{1,0:T(8,128)(2,1)S(1)}, u32[]{:S(2)}, u32[]{:S(2)}) collective-permute-start(bf16[64,256]{1,0:T(8,128)(2,1)S(1)} %collective-permute-done.14), channel_id=1, source_target_pairs={{0,30},{2,0},{4,2},{6,4},{8,6},{10,8},{12,10},{14,12},{16,14},{18,... | collective-permute-start | bytes 98312 | tf_op jit(solution)/shard_map/ppermute | solution.py:207
  191.2 2.0 collective-permute-start.9
  193.1 4.6 %collective-permute-start.16 = (bf16[64,256]{1,0:T(8,128)(2,1)S(1)}, bf16[64,256]{1,0:T(8,128)(2,1)S(1)}, u32[]{:S(2)}, u32[]{:S(2)}) collective-permute-start(bf16[64,256]{1,0:T(8,128)(2,1)S(1)} %collective-permute-done.15), channel_id=1, source_target_pairs={{0,30},{2,0},{4,2},{6,4},{8,6},{10,8},{12,10},{14,12},{16,14},{18,... | collective-permute-start | bytes 98312 | tf_op jit(solution)/shard_map/ppermute | solution.py:207
  197.8 2.0 collective-permute-start.10
  199.8 7.9 %collective-permute-start.18 = (bf16[1024,128]{1,0:T(8,128)(2,1)S(1)}, bf16[1024,128]{1,0:T(8,128)(2,1)S(1)}, u32[]{:S(2)}, u32[]{:S(2)}) collective-permute-start(bf16[1024,128]{1,0:T(8,128)(2,1)S(1)} %get-tuple-element.18), channel_id=1, source_target_pairs={{0,1},{1,0},{2,3},{3,2},{4,5},{5,4},{6,7},{7,6},{8,9},{9,8},{10,11... | collective-permute-start | bytes 786440 | tf_op jit(solution)/shard_map/ppermute | solution.py:31
  207.7 4.9 %collective-permute-start.17 = (bf16[64,256]{1,0:T(8,128)(2,1)S(1)}, bf16[64,256]{1,0:T(8,128)(2,1)S(1)}, u32[]{:S(2)}, u32[]{:S(2)}) collective-permute-start(bf16[64,256]{1,0:T(8,128)(2,1)S(1)} %collective-permute-done.16), channel_id=1, source_target_pairs={{0,30},{2,0},{4,2},{6,4},{8,6},{10,8},{12,10},{14,12},{16,14},{18,... | collective-permute-start | bytes 98312 | tf_op jit(solution)/shard_map/ppermute | solution.py:207
  214.3 13.4 %all_to_all.26 = bf16[16,32,128]{2,1,0:T(8,128)(2,1)S(1)} all-to-all(bf16[16,32,128]{2,1,0:T(8,128)(2,1)S(1)} %bitcast.104), channel_id=1, replica_groups=mesh['grp'=2,'dp'=8,'kv'=16,'tp'=2] {'dp','tp'}, dimensions={0} | all-to-all | bytes 262144 | tf_op jit(solution)/shard_map/all_to_all | solution.py:215
  (180 shorter events, 11.8 us)
Async XLA Ops:
  0.0 65.0 %copy-start = (f32[2,16,64,128]{3,2,1,0:T(8,128)S(1)}, f32[2,16,64,128]{3,2,1,0:T(8,128)}, u32[]{:S(2)}) copy-start(f32[2,16,64,128]{3,2,1,0:T(8,128)} %param.44) | copy-start | bytes 3145732
  3.7 47.1 %copy-start.10 = (f32[2,128,16]{1,2,0:T(8,128)S(1)}, f32[2,128,16]{1,2,0:T(8,128)}, u32[]{:S(2)}) copy-start(f32[2,128,16]{1,2,0:T(8,128)} %param.42) | copy-start | bytes 49156
  5.0 46.0 %copy-start.20 = (s32[2]{0:T(128)S(1)}, s32[2]{0:T(128)}, u32[]{:S(2)}) copy-start(s32[2]{0:T(128)} %param.43) | copy-start | bytes 28
  5.1 46.1 %copy-start.21 = (f32[16]{0:T(128)S(1)}, f32[16]{0:T(128)}, u32[]{:S(2)}) copy-start(f32[16]{0:T(128)} %param.39) | copy-start | bytes 196
  5.1 46.1 %copy-start.8 = (bf16[2,128,512]{2,1,0:T(8,128)(2,1)S(1)}, bf16[2,128,512]{2,1,0:T(8,128)(2,1)}, u32[]{:S(2)}) copy-start(bf16[2,128,512]{2,1,0:T(8,128)(2,1)} %param.41) | copy-start | bytes 786436
  5.3 46.1 %copy-start.5 = (bf16[2,128,1024]{2,1,0:T(8,128)(2,1)S(1)}, bf16[2,128,1024]{2,1,0:T(8,128)(2,1)}, u32[]{:S(2)}) copy-start(bf16[2,128,1024]{2,1,0:T(8,128)(2,1)} %param.40) | copy-start | bytes 1572868
  6.7 56.4 %all-to-all-start = ((bf16[16,2,3200]{2,1,0:T(2,128)(2,1)}), bf16[16,2,3200]{2,1,0:T(2,128)(2,1)S(1)}, u32[]{:S(2)}, u32[]{:S(2)}) async-start(bf16[16,2,3200]{2,1,0:T(2,128)(2,1)} %concatenate.58), calls=%async_computation | async-start | bytes 409600 | tf_op jit(solution)/shard_map/all_to_all | solution.py:101
  51.4 12.7 %copy-start.18 = (f32[16]{0:T(128)S(1)}, f32[16]{0:T(128)}, u32[]{:S(2)}) copy-start(f32[16]{0:T(128)} %param.38) | copy-start | bytes 196
  51.7 12.7 %copy-start.12 = (bf16[2,3,1024]{2,0,1:T(2,128)(2,1)S(1)}, bf16[2,3,1024]{2,0,1:T(2,128)(2,1)}, u32[]{:S(2)}) copy-start(bf16[2,3,1024]{2,0,1:T(2,128)(2,1)} %param.35) | copy-start | bytes 36868
  64.6 14.1 %copy-start.2 = (bf16[1024,256]{1,0:T(8,128)(2,1)S(1)}, bf16[1024,256]{1,0:T(8,128)(2,1)}, u32[]{:S(2)}) copy-start(bf16[1024,256]{1,0:T(8,128)(2,1)} %param.46) | copy-start | bytes 1572868
  68.1 26.9 %all-to-all-start.1 = ((bf16[32,2,1152]{2,1,0:T(2,128)(2,1)}), bf16[32,2,1152]{2,1,0:T(2,128)(2,1)S(1)}, u32[]{:S(2)}, u32[]{:S(2)}) async-start(bf16[32,2,1152]{2,1,0:T(2,128)(2,1)} %broadcast_in_dim.23), calls=%async_computation.1 | async-start | bytes 294912 | tf_op jit(solution)/shard_map/all_to_all | solution.py:24
  78.8 17.2 %collective-permute-start = (bf16[1024,128]{1,0:T(8,128)(2,1)S(1)}, bf16[1024,128]{1,0:T(8,128)(2,1)S(1)}, u32[]{:S(2)}, u32[]{:S(2)}) collective-permute-start(bf16[1024,128]{1,0:T(8,128)(2,1)S(1)} %get-tuple-element.16), channel_id=1, source_target_pairs={{0,1},{1,0},{2,3},{3,2},{4,5},{5,4},{6,7},{7,6},{8,9},{9,8},{10,11... | collective-permute-start | bytes 786440 | tf_op jit(solution)/shard_map/ppermute | solution.py:31
  96.8 17.8 %all-to-all-start.2 = ((bf16[16,32,128]{2,1,0:T(8,128)(2,1)}), bf16[16,32,128]{2,1,0:T(8,128)(2,1)S(1)}, u32[]{:S(2)}, u32[]{:S(2)}) async-start(bf16[16,32,128]{2,1,0:T(8,128)(2,1)} %broadcast_in_dim.24), calls=%async_computation.2 | async-start | bytes 262144 | tf_op jit(solution)/shard_map/all_to_all | solution.py:24
  105.8 4.6 %collective-permute-start.2 = (f32[128]{0:T(128)S(1)}, f32[128]{0:T(128)S(1)}, u32[]{:S(2)}, u32[]{:S(2)}) collective-permute-start(f32[128]{0:T(128)S(1)} %copy-done.19), channel_id=1, source_target_pairs={{0,1},{1,0},{2,3},{3,2},{4,5},{5,4},{6,7},{7,6},{8,9},{9,8},{10,11... | collective-permute-start | bytes 1544 | tf_op jit(solution)/shard_map/ppermute | solution.py:31
  108.1 6.8 %collective-permute-start.1 = (bf16[128,1024]{1,0:T(8,128)(2,1)S(1)}, bf16[128,1024]{1,0:T(8,128)(2,1)S(1)}, u32[]{:S(2)}, u32[]{:S(2)}) collective-permute-start(bf16[128,1024]{1,0:T(8,128)(2,1)S(1)} %get-tuple-element.14), channel_id=1, source_target_pairs={{0,1},{1,0},{2,3},{3,2},{4,5},{5,4},{6,7},{7,6},{8,9},{9,8},{10,11... | collective-permute-start | bytes 786440 | tf_op jit(solution)/shard_map/ppermute | solution.py:31
  115.3 84.4 %copy-start.4 = (bf16[2048,128]{1,0:T(8,128)(2,1)S(1)}, bf16[2048,128]{1,0:T(8,128)(2,1)}, u32[]{:S(2)}) copy-start(bf16[2048,128]{1,0:T(8,128)(2,1)} %param.49) | copy-start | bytes 1572868
  152.3 5.9 %collective-permute-start.3 = (bf16[64,256]{1,0:T(8,128)(2,1)S(1)}, bf16[64,256]{1,0:T(8,128)(2,1)S(1)}, u32[]{:S(2)}, u32[]{:S(2)}) collective-permute-start(bf16[64,256]{1,0:T(8,128)(2,1)S(1)} %fusion.25), channel_id=1, source_target_pairs={{0,2},{2,4},{4,6},{6,8},{8,10},{10,12},{12,14},{14,16},{16,18},{18... | collective-permute-start | bytes 98312 | tf_op jit(solution)/shard_map/ppermute | solution.py:205
  158.2 6.6 %collective-permute-start.4 = (bf16[64,256]{1,0:T(8,128)(2,1)S(1)}, bf16[64,256]{1,0:T(8,128)(2,1)S(1)}, u32[]{:S(2)}, u32[]{:S(2)}) collective-permute-start(bf16[64,256]{1,0:T(8,128)(2,1)S(1)} %collective-permute-done.3), channel_id=1, source_target_pairs={{0,2},{2,4},{4,6},{6,8},{8,10},{10,12},{12,14},{14,16},{16,18},{18... | collective-permute-start | bytes 98312 | tf_op jit(solution)/shard_map/ppermute | solution.py:205
  160.2 6.6 %collective-permute-start.11 = (bf16[64,256]{1,0:T(8,128)(2,1)S(1)}, bf16[64,256]{1,0:T(8,128)(2,1)S(1)}, u32[]{:S(2)}, u32[]{:S(2)}) collective-permute-start(bf16[64,256]{1,0:T(8,128)(2,1)S(1)} %fusion.25), channel_id=1, source_target_pairs={{0,30},{2,0},{4,2},{6,4},{8,6},{10,8},{12,10},{14,12},{16,14},{18,... | collective-permute-start | bytes 98312 | tf_op jit(solution)/shard_map/ppermute | solution.py:207
  164.8 6.6 %collective-permute-start.5 = (bf16[64,256]{1,0:T(8,128)(2,1)S(1)}, bf16[64,256]{1,0:T(8,128)(2,1)S(1)}, u32[]{:S(2)}, u32[]{:S(2)}) collective-permute-start(bf16[64,256]{1,0:T(8,128)(2,1)S(1)} %collective-permute-done.4), channel_id=1, source_target_pairs={{0,2},{2,4},{4,6},{6,8},{8,10},{10,12},{12,14},{14,16},{16,18},{18... | collective-permute-start | bytes 98312 | tf_op jit(solution)/shard_map/ppermute | solution.py:205
  166.8 6.6 %collective-permute-start.12 = (bf16[64,256]{1,0:T(8,128)(2,1)S(1)}, bf16[64,256]{1,0:T(8,128)(2,1)S(1)}, u32[]{:S(2)}, u32[]{:S(2)}) collective-permute-start(bf16[64,256]{1,0:T(8,128)(2,1)S(1)} %collective-permute-done.11), channel_id=1, source_target_pairs={{0,30},{2,0},{4,2},{6,4},{8,6},{10,8},{12,10},{14,12},{16,14},{18,... | collective-permute-start | bytes 98312 | tf_op jit(solution)/shard_map/ppermute | solution.py:207
  171.4 6.6 %collective-permute-start.6 = (bf16[64,256]{1,0:T(8,128)(2,1)S(1)}, bf16[64,256]{1,0:T(8,128)(2,1)S(1)}, u32[]{:S(2)}, u32[]{:S(2)}) collective-permute-start(bf16[64,256]{1,0:T(8,128)(2,1)S(1)} %collective-permute-done.5), channel_id=1, source_target_pairs={{0,2},{2,4},{4,6},{6,8},{8,10},{10,12},{12,14},{14,16},{16,18},{18... | collective-permute-start | bytes 98312 | tf_op jit(solution)/shard_map/ppermute | solution.py:205
  173.4 6.6 %collective-permute-start.13 = (bf16[64,256]{1,0:T(8,128)(2,1)S(1)}, bf16[64,256]{1,0:T(8,128)(2,1)S(1)}, u32[]{:S(2)}, u32[]{:S(2)}) collective-permute-start(bf16[64,256]{1,0:T(8,128)(2,1)S(1)} %collective-permute-done.12), channel_id=1, source_target_pairs={{0,30},{2,0},{4,2},{6,4},{8,6},{10,8},{12,10},{14,12},{16,14},{18,... | collective-permute-start | bytes 98312 | tf_op jit(solution)/shard_map/ppermute | solution.py:207
  178.0 6.6 %collective-permute-start.7 = (bf16[64,256]{1,0:T(8,128)(2,1)S(1)}, bf16[64,256]{1,0:T(8,128)(2,1)S(1)}, u32[]{:S(2)}, u32[]{:S(2)}) collective-permute-start(bf16[64,256]{1,0:T(8,128)(2,1)S(1)} %collective-permute-done.6), channel_id=1, source_target_pairs={{0,2},{2,4},{4,6},{6,8},{8,10},{10,12},{12,14},{14,16},{16,18},{18... | collective-permute-start | bytes 98312 | tf_op jit(solution)/shard_map/ppermute | solution.py:205
  180.0 6.6 %collective-permute-start.14 = (bf16[64,256]{1,0:T(8,128)(2,1)S(1)}, bf16[64,256]{1,0:T(8,128)(2,1)S(1)}, u32[]{:S(2)}, u32[]{:S(2)}) collective-permute-start(bf16[64,256]{1,0:T(8,128)(2,1)S(1)} %collective-permute-done.13), channel_id=1, source_target_pairs={{0,30},{2,0},{4,2},{6,4},{8,6},{10,8},{12,10},{14,12},{16,14},{18,... | collective-permute-start | bytes 98312 | tf_op jit(solution)/shard_map/ppermute | solution.py:207
  184.6 6.6 %collective-permute-start.8 = (bf16[64,256]{1,0:T(8,128)(2,1)S(1)}, bf16[64,256]{1,0:T(8,128)(2,1)S(1)}, u32[]{:S(2)}, u32[]{:S(2)}) collective-permute-start(bf16[64,256]{1,0:T(8,128)(2,1)S(1)} %collective-permute-done.7), channel_id=1, source_target_pairs={{0,2},{2,4},{4,6},{6,8},{8,10},{10,12},{12,14},{14,16},{16,18},{18... | collective-permute-start | bytes 98312 | tf_op jit(solution)/shard_map/ppermute | solution.py:205
  186.5 6.6 %collective-permute-start.15 = (bf16[64,256]{1,0:T(8,128)(2,1)S(1)}, bf16[64,256]{1,0:T(8,128)(2,1)S(1)}, u32[]{:S(2)}, u32[]{:S(2)}) collective-permute-start(bf16[64,256]{1,0:T(8,128)(2,1)S(1)} %collective-permute-done.14), channel_id=1, source_target_pairs={{0,30},{2,0},{4,2},{6,4},{8,6},{10,8},{12,10},{14,12},{16,14},{18,... | collective-permute-start | bytes 98312 | tf_op jit(solution)/shard_map/ppermute | solution.py:207
  191.2 6.6 %collective-permute-start.9 = (bf16[64,256]{1,0:T(8,128)(2,1)S(1)}, bf16[64,256]{1,0:T(8,128)(2,1)S(1)}, u32[]{:S(2)}, u32[]{:S(2)}) collective-permute-start(bf16[64,256]{1,0:T(8,128)(2,1)S(1)} %collective-permute-done.8), channel_id=1, source_target_pairs={{0,2},{2,4},{4,6},{6,8},{8,10},{10,12},{12,14},{14,16},{16,18},{18... | collective-permute-start | bytes 98312 | tf_op jit(solution)/shard_map/ppermute | solution.py:205
  193.1 14.6 %collective-permute-start.16 = (bf16[64,256]{1,0:T(8,128)(2,1)S(1)}, bf16[64,256]{1,0:T(8,128)(2,1)S(1)}, u32[]{:S(2)}, u32[]{:S(2)}) collective-permute-start(bf16[64,256]{1,0:T(8,128)(2,1)S(1)} %collective-permute-done.15), channel_id=1, source_target_pairs={{0,30},{2,0},{4,2},{6,4},{8,6},{10,8},{12,10},{14,12},{16,14},{18,... | collective-permute-start | bytes 98312 | tf_op jit(solution)/shard_map/ppermute | solution.py:207
  197.8 14.9 %collective-permute-start.10 = (bf16[64,256]{1,0:T(8,128)(2,1)S(1)}, bf16[64,256]{1,0:T(8,128)(2,1)S(1)}, u32[]{:S(2)}, u32[]{:S(2)}) collective-permute-start(bf16[64,256]{1,0:T(8,128)(2,1)S(1)} %collective-permute-done.9), channel_id=1, source_target_pairs={{0,2},{2,4},{4,6},{6,8},{8,10},{10,12},{12,14},{14,16},{16,18},{18... | collective-permute-start | bytes 98312 | tf_op jit(solution)/shard_map/ppermute | solution.py:205
  199.8 14.1 %collective-permute-start.18 = (bf16[1024,128]{1,0:T(8,128)(2,1)S(1)}, bf16[1024,128]{1,0:T(8,128)(2,1)S(1)}, u32[]{:S(2)}, u32[]{:S(2)}) collective-permute-start(bf16[1024,128]{1,0:T(8,128)(2,1)S(1)} %get-tuple-element.18), channel_id=1, source_target_pairs={{0,1},{1,0},{2,3},{3,2},{4,5},{5,4},{6,7},{7,6},{8,9},{9,8},{10,11... | collective-permute-start | bytes 786440 | tf_op jit(solution)/shard_map/ppermute | solution.py:31
  207.7 5.9 %collective-permute-start.17 = (bf16[64,256]{1,0:T(8,128)(2,1)S(1)}, bf16[64,256]{1,0:T(8,128)(2,1)S(1)}, u32[]{:S(2)}, u32[]{:S(2)}) collective-permute-start(bf16[64,256]{1,0:T(8,128)(2,1)S(1)} %collective-permute-done.16), channel_id=1, source_target_pairs={{0,30},{2,0},{4,2},{6,4},{8,6},{10,8},{12,10},{14,12},{16,14},{18,... | collective-permute-start | bytes 98312 | tf_op jit(solution)/shard_map/ppermute | solution.py:207
  (12 other events, 72.5 us)
